TPU v7x, 32 devices: a whole 2x2x4 slice. The times are simulated.
32 devices in a mesh: ep: 32 (over z, y, x, core).
Axes of the slice: x: 2, y: 2, z: 4, core: 2. Of those that a mesh axis runs over, the one named last changes fastest.
Arguments:
- tokens: bfloat16 [32, 2048], P('ep'), may hold values from -6 to 6
- mixer_gain: float32 [2048], replicated, may hold values from 0.1 to 1.9
- query_weight: bfloat16 [2048, 2048], P(None, 'ep'), may hold values from -0.125 to 0.125
- key_weight: bfloat16 [2048, 2048], P(None, 'ep'), may hold values from -0.125 to 0.125
- value_weight: bfloat16 [2048, 2048], P(None, 'ep'), may hold values from -0.125 to 0.125
- outgate_weight: bfloat16 [2048, 2048], P(None, 'ep'), may hold values from -0.125 to 0.125
- input_weight: bfloat16 [2048, 4], replicated, may hold values from -0.125 to 0.125
- forget_weight: bfloat16 [2048, 4], replicated, may hold values from -0.125 to 0.125
- forget_bias: float32 [4], replicated, may hold values from 0 to 4
- memory_matrix: float32 [32, 4, 512, 512], P('ep'), may hold values from -0.3 to 0.3
- memory_norm: float32 [32, 4, 512], P('ep'), may hold values from -0.3 to 0.3
- memory_max: float32 [32, 4], P('ep'), may hold values from -2 to 2
- mixer_out: bfloat16 [2048, 2048], P(None, 'ep'), may hold values from -0.125 to 0.125
- expert_gain: float32 [2048], replicated, may hold values from 0.1 to 1.9
- expert_gate: bfloat16 [32, 2048, 1024], P('ep'), may hold values from -0.125 to 0.125
- expert_up: bfloat16 [32, 2048, 1024], P('ep'), may hold values from -0.125 to 0.125
- expert_down: bfloat16 [32, 1024, 2048], P('ep'), may hold values from -0.1875 to 0.1875
- route_group: int32 [32], P('ep'), may hold values from 0 to 3
- route_member: int32 [32, 2], P('ep'), may hold values from 0 to 7, as said below
- group_weight: float32 [32], P('ep'), may hold values from 0.25 to 1
- member_weight: float32 [32, 2], P('ep'), may hold values from 0.1 to 1
Outputs:
- layer_out: bfloat16 [32, 2048], P('ep')
- next_matrix: float32 [32, 4, 512, 512], P('ep')
- next_norm: float32 [32, 4, 512], P('ep')
- next_max: float32 [32, 4], P('ep')
Inputs may be any that keep to these rules, and one draw needn't show every extreme that they name: A row's 2 experts, numbered route_group * 8 + route_member, are different members of the one group that route_group names. No expert is named by more than 4 rows in all, and one expert is named by exactly 4 rows.
All inputs are finite; a program needn't handle non-finite values.
Results may differ from a plain program's by a relative error of at most 0.013.
Values may be sent and summed in bfloat16 or wider, within the bound.
A program may use at most 64 MiB of HBM per device.

v0:
```python
import jax
import jax.numpy as jnp
from jax import lax
from jax.sharding import PartitionSpec as P

GROUPS = 4
CAPACITY = 4


norm_eps = 1e-06


def root_norm(values, gain):
    return values * lax.rsqrt(jnp.mean(values * values, axis=-1, keepdims=True) + norm_eps) * gain


def run_expert(slot_rows, gate_mat, up_mat, down_mat):
    gate_part = jnp.dot(slot_rows, gate_mat, preferred_element_type=jnp.float32)
    up_part = jnp.dot(slot_rows, up_mat, preferred_element_type=jnp.float32)
    hidden = (jax.nn.silu(gate_part) * up_part).astype(jnp.bfloat16)
    return jnp.dot(hidden, down_mat, preferred_element_type=jnp.float32).astype(jnp.bfloat16)


def local(
    tokens,
    mixer_gain,
    query_weight,
    key_weight,
    value_weight,
    outgate_weight,
    input_weight,
    forget_weight,
    forget_bias,
    memory_matrix,
    memory_norm,
    memory_max,
    mixer_out,
    expert_gain,
    expert_gate,
    expert_up,
    expert_down,
    route_group,
    route_member,
    group_weight,
    member_weight,
):
    devices = lax.axis_size("ep")
    local_rows = tokens.shape[0]
    width = tokens.shape[1]
    columns = query_weight.shape[1]
    heads = memory_matrix.shape[1]
    head_dim = memory_matrix.shape[2]
    members = devices * expert_gate.shape[0] // GROUPS
    stacked = jnp.concatenate([query_weight, key_weight, value_weight, outgate_weight], axis=1)
    piece = lax.all_gather(tokens, "ep", axis=0, tiled=True)
    normed = root_norm(piece.astype(jnp.float32), mixer_gain).astype(jnp.bfloat16)
    result = jnp.dot(normed, stacked, preferred_element_type=jnp.float32).astype(jnp.bfloat16)
    result = result.reshape(piece.shape[0], 4, columns)
    parts = lax.all_to_all(result, "ep", split_axis=0, concat_axis=2, tiled=True)
    resid = tokens.astype(jnp.float32)
    own_normed = root_norm(resid, mixer_gain).astype(jnp.bfloat16)
    input_pre = jnp.dot(own_normed, input_weight, preferred_element_type=jnp.float32)
    forget_pre = (
        jnp.dot(own_normed, forget_weight, preferred_element_type=jnp.float32) + forget_bias
    )
    log_forget = jax.nn.log_sigmoid(forget_pre)
    next_max = jnp.maximum(log_forget + memory_max, input_pre)
    keep = jnp.exp(log_forget + memory_max - next_max)
    admit = jnp.exp(input_pre - next_max)
    query_heads = parts[:, 0].astype(jnp.float32).reshape(local_rows, heads, head_dim)
    key_heads = parts[:, 1].astype(jnp.float32).reshape(local_rows, heads, head_dim) * head_dim ** (
        -0.5
    )
    value_heads = parts[:, 2].astype(jnp.float32).reshape(local_rows, heads, head_dim)
    carried = jnp.einsum(
        "shij,shj->shi", memory_matrix, query_heads, precision=lax.Precision.HIGHEST
    )
    score = jnp.sum(key_heads * query_heads, axis=-1)
    numer = keep[..., None] * carried + (admit * score)[..., None] * value_heads
    denom = keep * jnp.sum(memory_norm * query_heads, axis=-1) + admit * score
    head_out = numer / jnp.maximum(jnp.abs(denom), jnp.exp(-next_max))[..., None]
    gated = (
        head_out.reshape(local_rows, width) * jax.nn.sigmoid(parts[:, 3].astype(jnp.float32))
    ).astype(jnp.bfloat16)
    next_matrix = (
        keep[..., None, None] * memory_matrix
        + admit[..., None, None] * value_heads[..., :, None] * key_heads[..., None, :]
    )
    next_norm = keep[..., None] * memory_norm + admit[..., None] * key_heads
    proj_cols = jnp.dot(
        lax.all_gather(gated, "ep", axis=0, tiled=True),
        mixer_out,
        preferred_element_type=jnp.float32,
    ).astype(jnp.bfloat16)
    slot_index = jnp.arange(CAPACITY, dtype=jnp.int32)
    chosen_local = route_group[:, None] * members + route_member
    row_numbers = jnp.arange(local_rows, dtype=jnp.int32)
    local_weight = group_weight[:, None] * member_weight
    projected = lax.all_to_all(proj_cols, "ep", split_axis=0, concat_axis=1, tiled=True)
    middle = (resid + projected.astype(jnp.float32)).astype(jnp.bfloat16)
    expert_in = root_norm(middle.astype(jnp.float32), expert_gain).astype(jnp.bfloat16)
    targets = jnp.arange(devices, dtype=jnp.int32)
    hit = jnp.any(chosen_local[:, :, None] == targets[None, None, :], axis=1)
    outgoing = jnp.where(hit.T[:, :, None], expert_in[None, :, :], jnp.zeros((), jnp.bfloat16))
    present = hit.T.astype(jnp.bfloat16)
    incoming, flags = (
        lax.all_to_all(outgoing, "ep", split_axis=0, concat_axis=0, tiled=True),
        lax.all_to_all(present, "ep", split_axis=0, concat_axis=0, tiled=True),
    )
    flat_rows = incoming.reshape(devices * local_rows, width)
    live = (flags.reshape(devices * local_rows) > 0.5).astype(jnp.int32)
    position = jnp.cumsum(live) - 1
    select = ((position[None, :] == slot_index[:, None]) & (live[None, :] > 0)).astype(jnp.bfloat16)
    slot_rows = jnp.dot(select, flat_rows, preferred_element_type=jnp.float32).astype(jnp.bfloat16)
    finished = run_expert(slot_rows, expert_gate[0], expert_up[0], expert_down[0])
    back_rows = jnp.dot(select.T, finished, preferred_element_type=jnp.float32).astype(jnp.bfloat16)
    returned = lax.all_to_all(
        back_rows.reshape(devices, local_rows, width), "ep", split_axis=0, concat_axis=0, tiled=True
    )
    picked = returned[chosen_local.T, row_numbers[None, :]]
    mixture = jnp.sum(local_weight.T[:, :, None] * picked.astype(jnp.float32), axis=0)
    layer_out = (middle.astype(jnp.float32) + mixture).astype(jnp.bfloat16)
    return (layer_out, next_matrix, next_norm, next_max)


def solution(mesh):
    placed = (
        P("ep", None),
        P(),
        P(None, "ep"),
        P(None, "ep"),
        P(None, "ep"),
        P(None, "ep"),
        P(),
        P(),
        P(),
        P("ep", None, None, None),
        P("ep", None, None),
        P("ep", None),
        P(None, "ep"),
        P(),
        P("ep", None, None),
        P("ep", None, None),
        P("ep", None, None),
        P("ep"),
        P("ep", None),
        P("ep"),
        P("ep", None),
    )
    return jax.shard_map(
        local,
        mesh=mesh,
        in_specs=placed,
        out_specs=(P("ep", None), P("ep", None, None, None), P("ep", None, None), P("ep", None)),
        check_vma=False,
    )
```

profile of v0, /device:TPU:0, one launch (start us, length us, event | category | flops | bytes accessed | tf_op | source)
XLA Modules:
  0.0 155.1 jit_solution(15445792464496646408)
XLA Ops:
  0.7 44.3 %all-gather = bf16[32,1,2048]{2,1,0:T(2,128)(2,1)S(1)} all-gather(bf16[1,1,2048]{2,1,0:T(2,128)(2,1)} %bitcast.134), channel_id=1, replica_groups=mesh['ep'=32] {'ep'}, dimensions={0}, use_global_device_ids=true | all-gather | bytes 135168 | tf_op jit(solution)/shard_map/all_gather | solution.py:55
  45.1 0.3 convert_element_type.241
  45.6 1.6 %convolution_convert_fusion.2 = bf16[32,256]{1,0:T(8,128)(2,1)S(1)} fusion(bf16[2048,64]{0,1:T(8,128)(2,1)} %param.26, bf16[2048,64]{0,1:T(8,128)(2,1)} %param.25, bf16[2048,64]{0,1:T(8,128)(2,1)} %param.24, bf16[2048,64]{0,1:T(8,128)(2,1)} %param.23, f32[32,1,2048]{2,1,0:T(1,128)S(1)} %convert_element_type.241, f32[2048]{0:T(1024)} %param.22, ...), kind=kOutput, calls=%fused_computation.14 | convolution fusion | flops 37953536 | bytes 1335424 | tf_op jit(solution)/shard_map/dot_general | solution.py:57
  47.3 0.7 reshape.614
  48.0 2.5 %all-to-all-start = ((bf16[32,2,128]{2,1,0:T(2,128)(2,1)}), bf16[32,2,128]{2,1,0:T(2,128)(2,1)S(1)}, u32[]{:S(2)}, u32[]{:S(2)}) async-start(bf16[32,2,128]{2,1,0:T(2,128)(2,1)} %reshape.614), calls=%async_computation | async-start | bytes 32768 | tf_op jit(solution)/shard_map/all_to_all | solution.py:59
  50.6 0.6 multiply_reduce_fusion.4
  53.8 3.9 %all-to-all-done = bf16[32,2,128]{2,1,0:T(2,128)(2,1)S(1)} async-done(((bf16[32,2,128]{2,1,0:T(2,128)(2,1)}), bf16[32,2,128]{2,1,0:T(2,128)(2,1)S(1)}, u32[]{:S(2)}, u32[]{:S(2)}) %all-to-all-start) | async-done | bytes 16416 | tf_op jit(solution)/shard_map/all_to_all | solution.py:59
  58.0 4.1 %fusion.6 = f32[4,1,512]{2,1,0:T(1,128)S(1)} fusion(bf16[4,512,1]{1,2,0:T(2,128)(2,1)S(1)} %bitcast.137, f32[1,4,512,512]{3,2,1,0:T(8,128)} %param.30), kind=kOutput, calls=%fused_computation.7 | convolution fusion | flops 12582912 | bytes 4206592 | tf_op jit(solution)/shard_map/shij,shj->shi/dot_general | solution.py:75
  62.2 0.8 multiply_reduce_fusion.3
  63.1 38.6 %all-gather.1 = bf16[32,1,2048]{2,1,0:T(2,128)(2,1)S(1)} all-gather(bf16[1,1,2048]{2,1,0:T(2,128)(2,1)S(1)} %convert_bitcast_fusion), channel_id=1, replica_groups=mesh['ep'=32] {'ep'}, dimensions={0}, use_global_device_ids=true | all-gather | bytes 135168 | tf_op jit(solution)/shard_map/all_gather | solution.py:91
  102.0 0.6 copy.45
  102.6 2.5 %all-to-all-start.1 = ((bf16[32,1,64]{2,1,0:T(2,128)(2,1)}), bf16[32,1,64]{2,1,0:T(2,128)(2,1)S(1)}, u32[]{:S(2)}, u32[]{:S(2)}) async-start(bf16[32,1,64]{2,1,0:T(2,128)(2,1)} %copy.45), calls=%async_computation.1 | async-start | bytes 32768 | tf_op jit(solution)/shard_map/all_to_all | solution.py:99
  105.4 0.7 copy.46
  106.1 6.2 %all-to-all-done.1 = bf16[32,1,64]{2,1,0:T(2,128)(2,1)S(1)} async-done(((bf16[32,1,64]{2,1,0:T(2,128)(2,1)}), bf16[32,1,64]{2,1,0:T(2,128)(2,1)S(1)}, u32[]{:S(2)}, u32[]{:S(2)}) %all-to-all-start.1) | async-done | bytes 4128 | tf_op jit(solution)/shard_map/all_to_all | solution.py:99
  112.3 2.6 %all-to-all-start.2 = ((bf16[32,1,1]{2,1,0:T(2,128)(2,1)}), bf16[32,1,1]{2,1,0:T(2,128)(2,1)S(1)}, u32[]{:S(2)}, u32[]{:S(2)}) async-start(bf16[32,1,1]{2,1,0:T(2,128)(2,1)} %copy.46), calls=%async_computation.2 | async-start | bytes 32768 | tf_op jit(solution)/shard_map/all_to_all | solution.py:108
  115.0 0.6 multiply_reduce_fusion.1
  116.6 0.5 broadcast.318
  117.1 1.4 reduce.34
  118.5 0.7 reshape.616
  119.2 2.8 %all-to-all-done.2 = bf16[32,1,1]{2,1,0:T(2,128)(2,1)S(1)} async-done(((bf16[32,1,1]{2,1,0:T(2,128)(2,1)}), bf16[32,1,1]{2,1,0:T(2,128)(2,1)S(1)}, u32[]{:S(2)}, u32[]{:S(2)}) %all-to-all-start.2) | async-done | bytes 96 | tf_op jit(solution)/shard_map/all_to_all | solution.py:108
  122.0 3.1 %all-to-all-start.3 = ((bf16[32,2,1024]{2,1,0:T(2,128)(2,1)}), bf16[32,2,1024]{2,1,0:T(2,128)(2,1)S(1)}, u32[]{:S(2)}, u32[]{:S(2)}) async-start(bf16[32,2,1024]{2,1,0:T(2,128)(2,1)} %reshape.616), calls=%async_computation.3 | async-start | bytes 262144 | tf_op jit(solution)/shard_map/all_to_all | solution.py:107
  125.1 0.7 compare_reduce_fusion
  125.9 7.4 %all-to-all-done.3 = bf16[32,2,1024]{2,1,0:T(2,128)(2,1)S(1)} async-done(((bf16[32,2,1024]{2,1,0:T(2,128)(2,1)}), bf16[32,2,1024]{2,1,0:T(2,128)(2,1)S(1)}, u32[]{:S(2)}, u32[]{:S(2)}) %all-to-all-start.3) | async-done | bytes 131104 | tf_op jit(solution)/shard_map/all_to_all | solution.py:107
  133.6 2.8 %fusion.4 = f32[4,1024]{1,0:T(4,128)S(1)} fusion(bf16[4,2048]{1,0:T(4,128)(2,1)S(1)} %convolution_convert_fusion.1, bf16[1,2048,1024]{2,1,0:T(8,128)(2,1)} %param.35), kind=kOutput, calls=%fused_computation.5 | convolution fusion | flops 16777216 | bytes 4227072 | tf_op jit(solution)/shard_map/dot_general | solution.py:18
  136.4 4.7 %fusion.9 = bf16[4,2048]{1,0:T(4,128)(2,1)S(1)} fusion(bf16[1,1024,2048]{2,1,0:T(8,128)(2,1)} %param.37, bf16[4,2048]{1,0:T(4,128)(2,1)S(1)} %convolution_convert_fusion.1, bf16[1,2048,1024]{2,1,0:T(8,128)(2,1)} %param.36, f32[4,1024]{1,0:T(4,128)S(1)} %fusion.4), kind=kOutput, calls=%fused_computation.12 | convolution fusion | flops 33587200 | bytes 8437760 | tf_op jit(solution)/shard_map/dot_general | solution.py:21
  141.4 0.7 reduce.35
  142.0 0.7 reshape.618
  142.8 2.6 %all-to-all-start.4 = ((bf16[32,2,1024]{2,1,0:T(2,128)(2,1)}), bf16[32,2,1024]{2,1,0:T(2,128)(2,1)S(1)}, u32[]{:S(2)}, u32[]{:S(2)}) async-start(bf16[32,2,1024]{2,1,0:T(2,128)(2,1)} %reshape.618), calls=%async_computation.4 | async-start | bytes 262144 | tf_op jit(solution)/shard_map/all_to_all | solution.py:117
  145.3 4.7 %multiply_add_fusion = f32[1,4,512,512]{3,2,1,0:T(8,128)} fusion(f32[1,4,512,512]{3,2,1,0:T(8,128)} %param.30, f32[4,512]{1,0:T(4,128)S(1)} %mul.289, f32[4,512]{1,0:T(4,128)S(1)} %get-tuple-element.15, f32[4]{0:T(128)S(1)} %fusion.68), kind=kLoop, calls=%fused_computation.9 | loop fusion | flops 3145728 | bytes 8405008 | tf_op jit(solution)/shard_map/add | solution.py:86
  150.1 3.5 %all-to-all-done.4 = bf16[32,2,1024]{2,1,0:T(2,128)(2,1)S(1)} async-done(((bf16[32,2,1024]{2,1,0:T(2,128)(2,1)}), bf16[32,2,1024]{2,1,0:T(2,128)(2,1)S(1)}, u32[]{:S(2)}, u32[]{:S(2)}) %all-to-all-start.4) | async-done | bytes 131104 | tf_op jit(solution)/shard_map/all_to_all | solution.py:117
  153.7 0.6 gather_fusion
  154.5 0.6 add_convert_fusion
  (65 shorter events, 3.1 us)
Async XLA Ops:
  0.6 101.1 %copy-start = (bf16[2048,64]{0,1:T(8,128)(2,1)S(1)}, bf16[2048,64]{0,1:T(8,128)(2,1)}, u32[]{:S(2)}) copy-start(bf16[2048,64]{0,1:T(8,128)(2,1)} %param.33) | copy-start | bytes 786436
  0.6 49.9 %copy-start.1 = (bf16[1,2048]{1,0:T(2,128)(2,1)S(1)}, bf16[1,2048]{1,0:T(2,128)(2,1)}, u32[]{:S(2)}) copy-start(bf16[1,2048]{1,0:T(2,128)(2,1)} %param.21) | copy-start | bytes 12292
  0.7 52.7 %copy-start.2 = (f32[2048]{0:T(1024)S(1)}, f32[2048]{0:T(1024)}, u32[]{:S(2)}) copy-start(f32[2048]{0:T(1024)} %param.22) | copy-start | bytes 24580
  0.7 51.2 %copy-start.8 = (s32[1,2]{1,0:T(1,128)S(1)}, s32[1,2]{1,0:T(1,128)}, u32[]{:S(2)}) copy-start(s32[1,2]{1,0:T(1,128)} %param.39) | copy-start | bytes 28
  0.7 52.7 %copy-start.9 = (f32[1,4]{1,0:T(1,128)S(1)}, f32[1,4]{1,0:T(1,128)}, u32[]{:S(2)}) copy-start(f32[1,4]{1,0:T(1,128)} %param.32) | copy-start | bytes 52
  0.7 52.7 %copy-start.10 = (f32[4]{0:T(128)S(1)}, f32[4]{0:T(128)}, u32[]{:S(2)}) copy-start(f32[4]{0:T(128)} %param.29) | copy-start | bytes 52
  0.7 52.7 %copy-start.6 = (bf16[2048,4]{0,1:T(4,128)(2,1)S(1)}, bf16[2048,4]{0,1:T(4,128)(2,1)}, u32[]{:S(2)}) copy-start(bf16[2048,4]{0,1:T(4,128)(2,1)} %param.28) | copy-start | bytes 49156
  0.7 52.9 %copy-start.7 = (bf16[2048,4]{0,1:T(4,128)(2,1)S(1)}, bf16[2048,4]{0,1:T(4,128)(2,1)}, u32[]{:S(2)}) copy-start(bf16[2048,4]{0,1:T(4,128)(2,1)} %param.27) | copy-start | bytes 49156
  0.7 53.0 %copy-start.11 = (f32[1,2]{1,0:T(1,128)S(1)}, f32[1,2]{1,0:T(1,128)}, u32[]{:S(2)}) copy-start(f32[1,2]{1,0:T(1,128)} %param.41) | copy-start | bytes 28
  45.5 16.6 %copy-start.3 = (f32[1,4,512]{2,1,0:T(4,128)S(1)}, f32[1,4,512]{2,1,0:T(4,128)}, u32[]{:S(2)}) copy-start(f32[1,4,512]{2,1,0:T(4,128)} %param.31) | copy-start | bytes 24580
  45.5 70.8 %copy-start.4 = (f32[2048]{0:T(1024)S(1)}, f32[2048]{0:T(1024)}, u32[]{:S(2)}) copy-start(f32[2048]{0:T(1024)} %param.34) | copy-start | bytes 24580
  48.0 9.7 %all-to-all-start = ((bf16[32,2,128]{2,1,0:T(2,128)(2,1)}), bf16[32,2,128]{2,1,0:T(2,128)(2,1)S(1)}, u32[]{:S(2)}, u32[]{:S(2)}) async-start(bf16[32,2,128]{2,1,0:T(2,128)(2,1)} %reshape.614), calls=%async_computation | async-start | bytes 32768 | tf_op jit(solution)/shard_map/all_to_all | solution.py:59
  53.7 82.7 %copy-start.5 = (f32[1,4]{1,0:T(1,128)}, f32[1,4]{1,0:T(1,128)S(1)}, u32[]{:S(2)}) copy-start(f32[1,4]{1,0:T(1,128)S(1)} %get-tuple-element.11) | copy-start | bytes 52
  102.6 9.7 %all-to-all-start.1 = ((bf16[32,1,64]{2,1,0:T(2,128)(2,1)}), bf16[32,1,64]{2,1,0:T(2,128)(2,1)S(1)}, u32[]{:S(2)}, u32[]{:S(2)}) async-start(bf16[32,1,64]{2,1,0:T(2,128)(2,1)} %copy.45), calls=%async_computation.1 | async-start | bytes 32768 | tf_op jit(solution)/shard_map/all_to_all | solution.py:99
  112.3 9.7 %all-to-all-start.2 = ((bf16[32,1,1]{2,1,0:T(2,128)(2,1)}), bf16[32,1,1]{2,1,0:T(2,128)(2,1)S(1)}, u32[]{:S(2)}, u32[]{:S(2)}) async-start(bf16[32,1,1]{2,1,0:T(2,128)(2,1)} %copy.46), calls=%async_computation.2 | async-start | bytes 32768 | tf_op jit(solution)/shard_map/all_to_all | solution.py:108
  122.0 11.3 %all-to-all-start.3 = ((bf16[32,2,1024]{2,1,0:T(2,128)(2,1)}), bf16[32,2,1024]{2,1,0:T(2,128)(2,1)S(1)}, u32[]{:S(2)}, u32[]{:S(2)}) async-start(bf16[32,2,1024]{2,1,0:T(2,128)(2,1)} %reshape.616), calls=%async_computation.3 | async-start | bytes 262144 | tf_op jit(solution)/shard_map/all_to_all | solution.py:107
  142.8 10.8 %all-to-all-start.4 = ((bf16[32,2,1024]{2,1,0:T(2,128)(2,1)}), bf16[32,2,1024]{2,1,0:T(2,128)(2,1)S(1)}, u32[]{:S(2)}, u32[]{:S(2)}) async-start(bf16[32,2,1024]{2,1,0:T(2,128)(2,1)} %reshape.618), calls=%async_computation.4 | async-start | bytes 262144 | tf_op jit(solution)/shard_map/all_to_all | solution.py:117
where the time goes:
time: 156 us; the launch traced here: 155 us
  blocking collectives  83 us (53%)
  waiting for transfers between devices  23.7 us (15%)
  matrix products  14.3 us (9%)
  starting transfers between devices  13.3 us (9%)
  other arithmetic  11.7 us (8%)
  local copies, waits for them, and re-layouts  5.47 us (4%)
  between operations  3.69 us (2%)
    all_gather x1, blocking collectives, local(): piece = lax.all_gather(tokens, 'ep', axis=0, tiled=True)  44.3 us
    all_gather x1, blocking collectives, local(): lax.all_gather(gated, 'ep', axis=0, tiled=True)  38.6 us
    all_to_all x1, waiting for transfers between devices, local(): lax.all_to_all(outgoing, 'ep', split_axis=0, concat_axis=0, tiled=True)  7.35 us
    all_to_all x1, waiting for transfers between devices, local(): lax.all_to_all(proj_cols, 'ep', split_axis=0, concat_axis=1, tiled=True)  6.21 us
    add x1, other arithmetic, local(): keep[..., None, None] * memory_matrix  4.74 us
    dot_general x1, matrix products, run_expert(): jnp.dot(hidden, down_mat, preferred_element_type=jnp.float32)  4.68 us
    dot_general x1, matrix products, local(): jnp.einsum('shij,shj->shi', memory_matrix, query_heads, precision=lax.Pre...  4.15 us
    all_to_all x1, waiting for transfers between devices, local(): lax.all_to_all(result, 'ep', split_axis=0, concat_axis=2, tiled=True)  3.87 us
  transfers between devices with their start and end apart: 5, of which 5 were waited for; matrix products, arithmetic and copies ran while one was open for 7% of the time, Pallas kernels for 0%

commit v1 on v0

v1 whole, which is shorter than its diff:
```python
import functools

import jax
import jax.numpy as jnp
from jax import lax
from jax.experimental import pallas as pl
from jax.experimental.pallas import tpu as pltpu
from jax.sharding import PartitionSpec as P

GROUPS = 4
LANES = 128
norm_eps = 1e-06
MESH = pl.DeviceIdType.MESH
NT = (((1,), (1,)), ((), ()))


def kernel(
    n,
    cols,
    members,
    tokens_ref,
    gain_ref,
    egain_ref,
    q_hbm,
    k_hbm,
    v_hbm,
    o_hbm,
    iw_ref,
    fw_ref,
    fb_ref,
    mem_hbm,
    norm_ref,
    max_ref,
    mo_hbm,
    gate_hbm,
    up_hbm,
    down_hbm,
    group_ref,
    member_ref,
    gw_ref,
    mw_ref,
    out_ref,
    nnorm_ref,
    nmax_ref,
    key_ref,
    av_ref,
    keep_ref,
    w_in,
    w_out,
    mem,
    mem_hi,
    mem_lo,
    w_gate,
    w_up,
    w_down,
    spread,
    row16,
    sb1,
    rb1,
    sb2,
    rb2,
    x2,
    sb3,
    rb3,
    sb4,
    rb4,
    sb5,
    rb5,
    flat,
    lhs,
    middle,
    load_sem,
    send_sem,
    recv_sem,
):
    me = lax.axis_index("ep")
    width = tokens_ref.shape[1]
    blocks = width // LANES
    heads, head_dim = norm_ref.shape
    pad4 = w_in.shape[0]
    f32 = jnp.float32
    bf16 = jnp.bfloat16

    loads = []
    for src, dst in (
        (q_hbm, w_in.at[pl.ds(0, cols)]),
        (k_hbm, w_in.at[pl.ds(cols, cols)]),
        (v_hbm, w_in.at[pl.ds(2 * cols, cols)]),
        (o_hbm, w_in.at[pl.ds(3 * cols, cols)]),
        (mem_hbm, mem),
        (mo_hbm, w_out),
        (gate_hbm, w_gate),
        (up_hbm, w_up),
        (down_hbm, w_down),
    ):
        copy = pltpu.make_async_copy(src, dst, load_sem.at[len(loads)])
        copy.start()
        loads.append(copy)

    barrier = pltpu.get_barrier_semaphore()

    def greet(i, carry):
        pl.semaphore_signal(
            barrier, inc=1, device_id=(lax.rem(me + i, n),), device_id_type=MESH
        )
        return carry

    lax.fori_loop(1, n, greet, 0)

    def send_all(phase, source, target):
        def one(i, carry):
            peer = lax.rem(me + i, n)
            pltpu.make_async_remote_copy(
                src_ref=source(peer),
                dst_ref=target.at[me],
                send_sem=send_sem.at[phase],
                recv_sem=recv_sem.at[phase],
                device_id=(peer,),
                device_id_type=MESH,
            ).start()
            return carry

        lax.fori_loop(1, n, one, 0)

    def whole(phase, target):
        view = target.at[pl.ds(0, n - 1)]
        return pltpu.make_async_remote_copy(
            src_ref=view,
            dst_ref=view,
            send_sem=send_sem.at[phase],
            recv_sem=recv_sem.at[phase],
            device_id=(lax.rem(me + 1, n),),
            device_id_type=MESH,
        )

    tok = tokens_ref[...].astype(f32)
    for s in range(blocks):
        row16[pl.ds(s, 1), :] = tok[:, s * LANES : (s + 1) * LANES]
    sb1[...] = row16[...].astype(bf16)
    rb1[pl.ds(me, 1)] = sb1[...][None]

    pl.semaphore_wait(barrier, n - 1)
    send_all(0, lambda peer: sb1, rb1)

    own = row16[...]
    scale = lax.rsqrt(
        jnp.sum(jnp.sum(own * own, axis=1, keepdims=True), axis=0, keepdims=True) / width + norm_eps
    )
    own_normed = (own * scale * gain_ref[...]).astype(bf16).astype(f32)
    pre_in = jnp.zeros((heads, LANES), f32)
    pre_forget = jnp.zeros((heads, LANES), f32)
    for s in range(blocks):
        part = own_normed[s : s + 1, :]
        span = slice(s * LANES, (s + 1) * LANES)
        pre_in += iw_ref[:, span].astype(f32) * part
        pre_forget += fw_ref[:, span].astype(f32) * part
    input_pre = jnp.sum(pre_in, axis=1, keepdims=True)
    head_index = lax.broadcasted_iota(jnp.int32, (heads, 1), 0)
    bias = jnp.zeros((heads, 1), f32)
    old_max = jnp.zeros((heads, 1), f32)
    for h in range(heads):
        bias = jnp.where(head_index == h, fb_ref[h], bias)
        old_max = jnp.where(head_index == h, max_ref[0, h], old_max)
    forget_pre = jnp.sum(pre_forget, axis=1, keepdims=True) + bias
    log_forget = -(
        jnp.maximum(-forget_pre, 0.0) + jnp.log1p(jnp.exp(-jnp.abs(forget_pre)))
    )
    next_max = jnp.maximum(log_forget + old_max, input_pre)
    keep = jnp.exp(log_forget + old_max - next_max)
    admit = jnp.exp(input_pre - next_max)
    diag = lax.broadcasted_iota(jnp.int32, (heads, heads), 0) == lax.broadcasted_iota(
        jnp.int32, (heads, heads), 1
    )
    nmax_ref[...] = jnp.sum(jnp.where(diag, next_max, 0.0), axis=0, keepdims=True)
    keep_ref[...] = jnp.broadcast_to(keep, (heads, LANES))

    r_index = lax.broadcasted_iota(jnp.int32, (pad4, head_dim), 0)
    j_index = lax.broadcasted_iota(jnp.int32, (pad4, head_dim), 1)
    if cols & (cols - 1) == 0:
        same = ((r_index ^ j_index) & (cols - 1)) == 0
    else:
        same = lax.rem(r_index, cols) == lax.rem(j_index, cols)
    spread[...] = jnp.where(same, 1.0, 0.0).astype(bf16)
    if pad4 != 4 * cols:
        w_in[pl.ds(4 * cols, pad4 - 4 * cols), :] = jnp.zeros((pad4 - 4 * cols, width), bf16)

    for copy in loads[:4]:
        copy.wait()
    whole(0, rb1).wait_recv()
    rows = rb1[...].astype(f32)
    squares = jnp.sum(jnp.sum(rows * rows, axis=2, keepdims=True), axis=1, keepdims=True) / width
    normed = rows * lax.rsqrt(squares + norm_eps) * gain_ref[...][None]
    flat[...] = normed.reshape(n * blocks, LANES)
    for s in range(blocks):
        lhs[:, s * LANES : (s + 1) * LANES] = flat[pl.ds(s, n, stride=blocks), :].astype(bf16)
    result = lax.dot_general(lhs[...], w_in[...], NT, preferred_element_type=f32)
    result = result.astype(bf16).astype(f32)
    for t in range(n):
        sb2[t] = result[t : t + 1, :]
    rb2[pl.ds(me, 1)] = sb2[pl.ds(me, 1)]
    send_all(1, lambda peer: sb2.at[peer], rb2)

    loads[4].wait()
    for h in range(heads):
        block = mem[h]
        high = block.astype(bf16)
        mem_hi[h] = high
        mem_lo[h] = (block - high.astype(f32)).astype(bf16)

    whole(1, rb2).wait_recv()
    for d in range(n):
        x2[pl.ds(d, 1), :] = rb2[d]
    got = x2[...]
    lane = lax.broadcasted_iota(jnp.int32, (n, pad4), 1)
    stacked = jnp.concatenate(
        [
            jnp.where((lane >= m * cols) & (lane < (m + 1) * cols), got, 0.0).astype(bf16)
            for m in range(4)
        ],
        axis=0,
    )
    wide = jnp.dot(stacked, spread[...], preferred_element_type=f32)
    per_head = n // heads
    wide = wide.reshape(4 * heads, per_head, head_dim)
    d_index = lax.broadcasted_iota(jnp.int32, (1, per_head, head_dim), 1)
    lane = lax.broadcasted_iota(jnp.int32, (1, per_head, head_dim), 2)
    here = (lane >= d_index * cols) & (lane < (d_index + 1) * cols)
    vectors = jnp.sum(jnp.where(here, wide, 0.0), axis=1)
    query = vectors[:heads]
    key = vectors[heads : 2 * heads] * head_dim ** (-0.5)
    value = vectors[2 * heads : 3 * heads]
    outgate = vectors[3 * heads :]
    query_bf = query.astype(bf16)
    carried = []
    for h in range(heads):
        both = lax.dot_general(
            query_bf, mem_hi[h], NT, preferred_element_type=f32
        ) + lax.dot_general(query_bf, mem_lo[h], NT, preferred_element_type=f32)
        carried.append(both[h : h + 1, :])
    carried = jnp.concatenate(carried, axis=0)
    score = jnp.sum(key * query, axis=1, keepdims=True)
    old_norm = norm_ref[...]
    numer = keep * carried + (admit * score) * value
    denom = keep * jnp.sum(old_norm * query, axis=1, keepdims=True) + admit * score
    head_out = numer / jnp.maximum(jnp.abs(denom), jnp.exp(-next_max))
    gated = head_out * jax.nn.sigmoid(outgate)
    per = head_dim // LANES
    for b in range(per):
        row16[pl.ds(b, heads, stride=per), :] = gated[:, b * LANES : (b + 1) * LANES]
    sb3[...] = row16[...].astype(bf16)
    rb3[pl.ds(me, 1)] = sb3[...][None]
    send_all(2, lambda peer: sb3, rb3)
    nnorm_ref[...] = keep * old_norm + admit * key
    key_ref[...] = key
    av_ref[...] = admit * value

    loads[5].wait()
    whole(2, rb3).wait_recv()
    flat[...] = rb3[...].astype(f32).reshape(n * blocks, LANES)
    for s in range(blocks):
        lhs[:, s * LANES : (s + 1) * LANES] = flat[pl.ds(s, n, stride=blocks), :].astype(bf16)
    proj = lax.dot_general(lhs[...], w_out[...], NT, preferred_element_type=f32)
    fold = LANES // cols
    piece = n // fold
    proj = proj.astype(bf16).astype(f32)
    sb4[...] = jnp.concatenate(
        [proj[f * piece : (f + 1) * piece, :] for f in range(fold)], axis=1
    ).astype(bf16)
    rb4[pl.ds(me, 1)] = sb4[...][None]
    send_all(3, lambda peer: sb4, rb4)
    flat[...] = rb1[...].astype(f32).reshape(n * blocks, LANES)

    whole(3, rb4).wait_recv()
    lane = lax.broadcasted_iota(jnp.int32, (piece, LANES), 1)
    squares = jnp.zeros((n, LANES), f32)
    for s in range(blocks):
        pieces = [rb4[s * fold + g].astype(f32) for g in range(fold)]
        parts = []
        for f in range(fold):
            made = pieces[0] if f == 0 else pltpu.roll(pieces[0], (-f * cols) % LANES, 1)
            for g in range(1, fold):
                moved = (
                    pieces[g] if g == f else pltpu.roll(pieces[g], ((g - f) * cols) % LANES, 1)
                )
                made = jnp.where(lane >= g * cols, moved, made)
            parts.append(made)
        projected = jnp.concatenate(parts, axis=0)
        mid = (flat[pl.ds(s, n, stride=blocks), :] + projected).astype(bf16).astype(f32)
        middle[:, s * LANES : (s + 1) * LANES] = mid
        squares += mid * mid
    inverse = lax.rsqrt(jnp.sum(squares, axis=1, keepdims=True) / width + norm_eps)
    for s in range(blocks):
        span = slice(s * LANES, (s + 1) * LANES)
        lhs[:, span] = (middle[:, span] * inverse * egain_ref[pl.ds(s, 1), :]).astype(bf16)
    for copy in loads[6:]:
        copy.wait()
    gate_part = jnp.dot(lhs[...], w_gate[...], preferred_element_type=f32)
    up_part = jnp.dot(lhs[...], w_up[...], preferred_element_type=f32)
    hidden = (gate_part / (1.0 + jnp.exp(-gate_part)) * up_part).astype(bf16)
    finished = jnp.dot(hidden, w_down[...], preferred_element_type=f32)
    for s in range(blocks):
        flat[pl.ds(s, n, stride=blocks), :] = finished[:, s * LANES : (s + 1) * LANES]
    sb5[...] = flat[...].astype(bf16).reshape(n, blocks, LANES)
    rb5[pl.ds(me, 1)] = sb5[pl.ds(me, 1)]
    send_all(4, lambda peer: sb5.at[peer], rb5)

    own_middle = middle[pl.ds(me, 1), :]
    for s in range(blocks):
        row16[pl.ds(s, 1), :] = own_middle[:, s * LANES : (s + 1) * LANES]
    whole(4, rb5).wait_recv()
    mixture = jnp.zeros((blocks, LANES), f32)
    for j in range(member_ref.shape[1]):
        chosen = group_ref[0] * members + member_ref[0, j]
        weight = gw_ref[0] * mw_ref[0, j]
        mixture += weight * rb5[chosen].astype(f32)
    row16[...] = row16[...] + mixture
    final = row16[...]
    for s in range(blocks):
        out_ref[:, s * LANES : (s + 1) * LANES] = final[s : s + 1, :].astype(bf16)
    whole(0, rb1).wait_send()
    whole(1, rb2).wait_send()
    whole(2, rb3).wait_send()
    whole(3, rb4).wait_send()
    whole(4, rb5).wait_send()


def local(
    tokens,
    mixer_gain,
    query_weight,
    key_weight,
    value_weight,
    outgate_weight,
    input_weight,
    forget_weight,
    forget_bias,
    memory_matrix,
    memory_norm,
    memory_max,
    mixer_out,
    expert_gain,
    expert_gate,
    expert_up,
    expert_down,
    route_group,
    route_member,
    group_weight,
    member_weight,
):
    n = lax.axis_size("ep")
    assert tokens.shape[0] == 1 and expert_gate.shape[0] == 1
    width = tokens.shape[1]
    cols = query_weight.shape[1]
    heads, head_dim = memory_matrix.shape[1:3]
    hidden = expert_gate.shape[2]
    blocks = width // LANES
    members = n * expert_gate.shape[0] // GROUPS
    pad4 = -(-4 * cols // LANES) * LANES
    fold = LANES // cols
    f32, bf16 = jnp.float32, jnp.bfloat16
    vmem = pl.BlockSpec(memory_space=pltpu.VMEM)
    smem = pl.BlockSpec(memory_space=pltpu.SMEM)
    anym = pl.BlockSpec(memory_space=pl.ANY)
    outs = pl.pallas_call(
        functools.partial(kernel, n, cols, members),
        out_shape=(
            jax.ShapeDtypeStruct((1, width), bf16),
            jax.ShapeDtypeStruct((heads, head_dim), f32),
            jax.ShapeDtypeStruct((1, heads), f32),
            jax.ShapeDtypeStruct((heads, head_dim), f32),
            jax.ShapeDtypeStruct((heads, head_dim), f32),
            jax.ShapeDtypeStruct((heads, LANES), f32),
        ),
        in_specs=[vmem] * 3
        + [anym] * 4
        + [vmem, vmem, smem, anym, vmem, smem, anym, anym, anym, anym]
        + [smem] * 4,
        out_specs=(vmem,) * 6,
        scratch_shapes=[
            pltpu.VMEM((pad4, width), bf16),
            pltpu.VMEM((cols, width), bf16),
            pltpu.VMEM((heads, head_dim, head_dim), f32),
            pltpu.VMEM((heads, head_dim, head_dim), bf16),
            pltpu.VMEM((heads, head_dim, head_dim), bf16),
            pltpu.VMEM((width, hidden), bf16),
            pltpu.VMEM((width, hidden), bf16),
            pltpu.VMEM((hidden, width), bf16),
            pltpu.VMEM((pad4, head_dim), bf16),
            pltpu.VMEM((blocks, LANES), f32),
            pltpu.VMEM((blocks, LANES), bf16),
            pltpu.VMEM((n, blocks, LANES), bf16),
            pltpu.VMEM((n, 1, pad4), f32),
            pltpu.VMEM((n, 1, pad4), f32),
            pltpu.VMEM((n, pad4), f32),
            pltpu.VMEM((blocks, LANES), bf16),
            pltpu.VMEM((n, blocks, LANES), bf16),
            pltpu.VMEM((n // fold, LANES), bf16),
            pltpu.VMEM((n, n // fold, LANES), bf16),
            pltpu.VMEM((n, blocks, LANES), bf16),
            pltpu.VMEM((n, blocks, LANES), bf16),
            pltpu.VMEM((n * blocks, LANES), f32),
            pltpu.VMEM((n, width), bf16),
            pltpu.VMEM((n, width), f32),
            pltpu.SemaphoreType.DMA((9,)),
            pltpu.SemaphoreType.DMA((5,)),
            pltpu.SemaphoreType.DMA((5,)),
        ],
        compiler_params=pltpu.CompilerParams(
            collective_id=0, has_side_effects=True, vmem_limit_bytes=48 * 1024 * 1024
        ),
    )(
        tokens,
        mixer_gain.reshape(blocks, LANES),
        expert_gain.reshape(blocks, LANES),
        query_weight.T,
        key_weight.T,
        value_weight.T,
        outgate_weight.T,
        input_weight.T,
        forget_weight.T,
        forget_bias,
        memory_matrix[0],
        memory_norm[0],
        memory_max,
        mixer_out.T,
        expert_gate[0],
        expert_up[0],
        expert_down[0],
        route_group,
        route_member,
        group_weight,
        member_weight,
    )
    layer_out, next_norm, next_max, key, value, keep = outs
    next_matrix = (
        keep[None, :, :1, None] * memory_matrix
        + value[None, :, :, None] * key[None, :, None, :]
    )
    return (layer_out, next_matrix, next_norm[None], next_max)


def solution(mesh):
    placed = (
        P("ep", None),
        P(),
        P(None, "ep"),
        P(None, "ep"),
        P(None, "ep"),
        P(None, "ep"),
        P(),
        P(),
        P(),
        P("ep", None, None, None),
        P("ep", None, None),
        P("ep", None),
        P(None, "ep"),
        P(),
        P("ep", None, None),
        P("ep", None, None),
        P("ep", None, None),
        P("ep"),
        P("ep", None),
        P("ep"),
        P("ep", None),
    )
    return jax.shard_map(
        local,
        mesh=mesh,
        in_specs=placed,
        out_specs=(P("ep", None), P("ep", None, None, None), P("ep", None, None), P("ep", None)),
        check_vma=False,
    )
```

time: 156 us -> 59.2 us (0.38)
  blocking collectives: 83 us -> 0 us
  Pallas kernels: 0 us -> 38.4 us
  waiting for transfers between devices: 23.7 us -> 0 us
  matrix products: 14.3 us -> 0 us
  starting transfers between devices: 13.3 us -> 0 us
  local copies, waits for them, and re-layouts: 5.47 us -> 15.6 us
  other arithmetic: 11.7 us -> 2.57 us
  between operations: 3.69 us -> 1.96 us
    all_gather x2 -> x0, blocking collectives: 83 us -> none  [the longest x1 44.3 us: local(): piece = lax.all_gather(tokens, 'ep', axis=0, tiled=True)]
    pallas_call x0 -> x1, Pallas kernels: none -> 38.4 us  [local(): pl.pallas_call(functools.partial(kernel, n, cols, members), out_shape=(ja...]
    all_to_all x5 -> x0, waiting for transfers between devices: 23.7 us -> none  [the longest x1 7.35 us: local(): lax.all_to_all(outgoing, 'ep', split_axis=0, concat_axis=0, tiled=True)]
    dot_general x9 -> x0, matrix products: 14.3 us -> none  [the longest x1 4.68 us: run_expert(): jnp.dot(hidden, down_mat, preferred_element_type=jnp.float32)]
    all_to_all x5 -> x0, starting transfers between devices: 13.3 us -> none  [the longest x1 3.06 us: local(): lax.all_to_all(outgoing, 'ep', split_axis=0, concat_axis=0, tiled=True)]
    unnamed x32 -> x35, local copies, waits for them, and re-layouts: 2.59 us -> 15.5 us
    reduce_sum x5 -> x0, other arithmetic: 2.33 us -> none  [the longest x3 1.41 us: root_norm(): jnp.mean(values * values, axis=-1, keepdims=True) + norm_eps]
    add x2 -> x1, other arithmetic: 4.75 us -> 2.57 us  [local(): keep[None, :, :1, None] * memory_matrix]
  transfers between devices with their start and end apart: 5 -> 0, of which waited for: 5 -> 0; matrix products, arithmetic and copies ran while one was open for 7% -> 0% of each run, Pallas kernels for 0% -> 0%
where the time goes in v1:
time: 59.2 us; the launch traced here: 58.5 us
  Pallas kernels  38.4 us (65%)
  local copies, waits for them, and re-layouts  15.6 us (26%)
  other arithmetic  2.57 us (4%)
  between operations  1.96 us (3%)
    pallas_call x1, Pallas kernels, local(): pl.pallas_call(functools.partial(kernel, n, cols, members), out_shape=(ja...  38.4 us
    unnamed x35, local copies, waits for them, and re-layouts  15.5 us
    add x1, other arithmetic, local(): keep[None, :, :1, None] * memory_matrix  2.57 us

profile of v1, /device:TPU:0, one launch (start us, length us, event | category | flops | bytes accessed | tf_op | source)
XLA Modules:
  0.0 58.5 jit_solution(15044458174180978957)
XLA Ops:
  1.9 0.0 copy-start
  1.9 2.2 %copy-done = f32[1,4,512,512]{3,2,1,0:T(8,128)S(1)} copy-done((f32[1,4,512,512]{3,2,1,0:T(8,128)S(1)}, f32[1,4,512,512]{3,2,1,0:T(8,128)}, u32[]{:S(2)}) %copy-start) | copy-done | bytes 4194328
  4.1 0.0 copy-start.1
  4.1 0.9 %copy-done.1 = bf16[2048,64]{0,1:T(8,128)(2,1)S(1)} copy-done((bf16[2048,64]{0,1:T(8,128)(2,1)S(1)}, bf16[2048,64]{0,1:T(8,128)(2,1)}, u32[]{:S(2)}) %copy-start.1) | copy-done | bytes 262168
  5.1 0.9 %copy-done.2 = bf16[2048,64]{0,1:T(8,128)(2,1)S(1)} copy-done((bf16[2048,64]{0,1:T(8,128)(2,1)S(1)}, bf16[2048,64]{0,1:T(8,128)(2,1)}, u32[]{:S(2)}) %copy-start.2) | copy-done | bytes 262168
  6.0 0.0 copy-start.3
  6.0 0.9 %copy-done.3 = bf16[2048,64]{0,1:T(8,128)(2,1)S(1)} copy-done((bf16[2048,64]{0,1:T(8,128)(2,1)S(1)}, bf16[2048,64]{0,1:T(8,128)(2,1)}, u32[]{:S(2)}) %copy-start.3) | copy-done | bytes 262168
  7.0 0.0 copy-start.4
  7.0 0.9 %copy-done.4 = bf16[2048,64]{0,1:T(8,128)(2,1)S(1)} copy-done((bf16[2048,64]{0,1:T(8,128)(2,1)S(1)}, bf16[2048,64]{0,1:T(8,128)(2,1)}, u32[]{:S(2)}) %copy-start.4) | copy-done | bytes 262168
  7.9 0.0 copy-start.5
  7.9 0.9 %copy-done.5 = bf16[2048,64]{0,1:T(8,128)(2,1)S(1)} copy-done((bf16[2048,64]{0,1:T(8,128)(2,1)S(1)}, bf16[2048,64]{0,1:T(8,128)(2,1)}, u32[]{:S(2)}) %copy-start.5) | copy-done | bytes 262168
  8.9 0.0 copy-start.6
  8.9 0.7 %copy-done.6 = bf16[2048,4]{0,1:T(4,128)(2,1)S(1)} copy-done((bf16[2048,4]{0,1:T(4,128)(2,1)S(1)}, bf16[2048,4]{0,1:T(4,128)(2,1)}, u32[]{:S(2)}) %copy-start.6) | copy-done | bytes 16408
  9.6 0.7 %copy-done.7 = bf16[2048,4]{0,1:T(4,128)(2,1)S(1)} copy-done((bf16[2048,4]{0,1:T(4,128)(2,1)S(1)}, bf16[2048,4]{0,1:T(4,128)(2,1)}, u32[]{:S(2)}) %copy-start.7) | copy-done | bytes 16408
  10.3 0.0 copy-start.8
  10.3 0.7 %copy-done.8 = bf16[1,2048]{1,0:T(2,128)(2,1)S(1)} copy-done((bf16[1,2048]{1,0:T(2,128)(2,1)S(1)}, bf16[1,2048]{1,0:T(2,128)(2,1)}, u32[]{:S(2)}) %copy-start.8) | copy-done | bytes 4120
  11.0 0.0 copy-start.9
  11.0 0.7 %copy-done.9 = f32[2048]{0:T(1024)S(1)} copy-done((f32[2048]{0:T(1024)S(1)}, f32[2048]{0:T(1024)}, u32[]{:S(2)}) %copy-start.9) | copy-done | bytes 8216
  11.7 0.0 copy-start.10
  11.7 0.7 %copy-done.10 = f32[2048]{0:T(1024)S(1)} copy-done((f32[2048]{0:T(1024)S(1)}, f32[2048]{0:T(1024)}, u32[]{:S(2)}) %copy-start.10) | copy-done | bytes 8216
  12.4 0.7 %copy-done.11 = f32[1,4,512]{2,1,0:T(4,128)S(1)} copy-done((f32[1,4,512]{2,1,0:T(4,128)S(1)}, f32[1,4,512]{2,1,0:T(4,128)}, u32[]{:S(2)}) %copy-start.11) | copy-done | bytes 8216
  13.1 0.0 copy-start.12
  13.1 0.7 %copy-done.12 = f32[4]{0:T(128)S(1)} copy-done((f32[4]{0:T(128)S(1)}, f32[4]{0:T(128)}, u32[]{:S(2)}) %copy-start.12) | copy-done | bytes 40
  13.8 0.7 %copy-done.13 = f32[1,4]{1,0:T(1,128)S(1)} copy-done((f32[1,4]{1,0:T(1,128)S(1)}, f32[1,4]{1,0:T(1,128)}, u32[]{:S(2)}) %copy-start.13) | copy-done | bytes 40
  14.4 0.7 %copy-done.14 = s32[1,2]{1,0:T(1,128)S(1)} copy-done((s32[1,2]{1,0:T(1,128)S(1)}, s32[1,2]{1,0:T(1,128)}, u32[]{:S(2)}) %copy-start.14) | copy-done | bytes 32
  15.1 0.7 %copy-done.15 = f32[1,2]{1,0:T(1,128)S(1)} copy-done((f32[1,2]{1,0:T(1,128)S(1)}, f32[1,2]{1,0:T(1,128)}, u32[]{:S(2)}) %copy-start.15) | copy-done | bytes 32
  15.7 38.4 %shard_map.228 = (bf16[1,2048]{1,0:T(2,128)(2,1)S(1)}, f32[4,512]{1,0:T(4,128)S(1)}, f32[1,4]{1,0:T(1,128)S(1)}, f32[4,512]{1,0:T(4,128)S(1)}, f32[4,512]{1,0:T(4,128)S(1)}, /*index=5*/f32[4,128]{1,0:T(4,128)S(1)}) custom-call(bf16[1,2048]{1,0:T(2,128)(2,1)S(1)} %copy-done.8, f32[16,128]{1,0:T(8,128)S(1)} %bitcast.23, f32[16,128]{1,0:T(8,128)S(1)} %bitcast.24, ...), custom_call_target="tpu_custom_call" | custom-call | tf_op jit(solution)/shard_map/pallas_call | solution.py:364
  54.1 0.1 slice_reduce_fusion
  54.2 2.6 %multiply_add_fusion = f32[1,4,512,512]{3,2,1,0:T(8,128)} fusion(f32[1,4,512,512]{3,2,1,0:T(8,128)S(1)} %copy-done, f32[4,512]{1,0:T(4,128)S(1)} %get-tuple-element.13, f32[4,512]{1,0:T(4,128)S(1)} %get-tuple-element.12, f32[4]{0:T(128)S(1)} %slice_reduce_fusion), kind=kLoop, calls=%fused_computation | loop fusion | flops 3145728 | bytes 8405008 | tf_op jit(solution)/shard_map/add | solution.py:436
  56.8 0.6 %copy.30 = bf16[1,2048]{1,0:T(2,128)(2,1)} copy(bf16[1,2048]{1,0:T(2,128)(2,1)S(1)} %get-tuple-element.20) | data formatting | bytes 8192
  57.4 0.6 %copy.31 = f32[1,4,512]{2,1,0:T(4,128)} copy(f32[1,4,512]{2,1,0:T(4,128)S(1)} %bitcast.26) | data formatting | bytes 16384
  58.0 0.5 copy.32
  (6 shorter events, 0.0 us)
Async XLA Ops:
  1.9 2.2 %copy-start = (f32[1,4,512,512]{3,2,1,0:T(8,128)S(1)}, f32[1,4,512,512]{3,2,1,0:T(8,128)}, u32[]{:S(2)}) copy-start(f32[1,4,512,512]{3,2,1,0:T(8,128)} %param.30) | copy-start | bytes 12582916
  4.1 0.9 %copy-start.1 = (bf16[2048,64]{0,1:T(8,128)(2,1)S(1)}, bf16[2048,64]{0,1:T(8,128)(2,1)}, u32[]{:S(2)}) copy-start(bf16[2048,64]{0,1:T(8,128)(2,1)} %param.23) | copy-start | bytes 786436
  5.1 0.9 %copy-start.2 = (bf16[2048,64]{0,1:T(8,128)(2,1)S(1)}, bf16[2048,64]{0,1:T(8,128)(2,1)}, u32[]{:S(2)}) copy-start(bf16[2048,64]{0,1:T(8,128)(2,1)} %param.24) | copy-start | bytes 786436
  6.0 0.9 %copy-start.3 = (bf16[2048,64]{0,1:T(8,128)(2,1)S(1)}, bf16[2048,64]{0,1:T(8,128)(2,1)}, u32[]{:S(2)}) copy-start(bf16[2048,64]{0,1:T(8,128)(2,1)} %param.25) | copy-start | bytes 786436
  7.0 0.9 %copy-start.4 = (bf16[2048,64]{0,1:T(8,128)(2,1)S(1)}, bf16[2048,64]{0,1:T(8,128)(2,1)}, u32[]{:S(2)}) copy-start(bf16[2048,64]{0,1:T(8,128)(2,1)} %param.26) | copy-start | bytes 786436
  7.9 0.9 %copy-start.5 = (bf16[2048,64]{0,1:T(8,128)(2,1)S(1)}, bf16[2048,64]{0,1:T(8,128)(2,1)}, u32[]{:S(2)}) copy-start(bf16[2048,64]{0,1:T(8,128)(2,1)} %param.33) | copy-start | bytes 786436
  8.9 0.7 %copy-start.6 = (bf16[2048,4]{0,1:T(4,128)(2,1)S(1)}, bf16[2048,4]{0,1:T(4,128)(2,1)}, u32[]{:S(2)}) copy-start(bf16[2048,4]{0,1:T(4,128)(2,1)} %param.27) | copy-start | bytes 49156
  9.6 0.7 %copy-start.7 = (bf16[2048,4]{0,1:T(4,128)(2,1)S(1)}, bf16[2048,4]{0,1:T(4,128)(2,1)}, u32[]{:S(2)}) copy-start(bf16[2048,4]{0,1:T(4,128)(2,1)} %param.28) | copy-start | bytes 49156
  10.3 0.7 %copy-start.8 = (bf16[1,2048]{1,0:T(2,128)(2,1)S(1)}, bf16[1,2048]{1,0:T(2,128)(2,1)}, u32[]{:S(2)}) copy-start(bf16[1,2048]{1,0:T(2,128)(2,1)} %tokens_ref.1) | copy-start | bytes 12292
  11.0 0.7 %copy-start.9 = (f32[2048]{0:T(1024)S(1)}, f32[2048]{0:T(1024)}, u32[]{:S(2)}) copy-start(f32[2048]{0:T(1024)} %param.22) | copy-start | bytes 24580
  11.7 0.7 %copy-start.10 = (f32[2048]{0:T(1024)S(1)}, f32[2048]{0:T(1024)}, u32[]{:S(2)}) copy-start(f32[2048]{0:T(1024)} %param.34) | copy-start | bytes 24580
  12.4 0.7 %copy-start.11 = (f32[1,4,512]{2,1,0:T(4,128)S(1)}, f32[1,4,512]{2,1,0:T(4,128)}, u32[]{:S(2)}) copy-start(f32[1,4,512]{2,1,0:T(4,128)} %param.31) | copy-start | bytes 24580
  13.1 0.7 %copy-start.12 = (f32[4]{0:T(128)S(1)}, f32[4]{0:T(128)}, u32[]{:S(2)}) copy-start(f32[4]{0:T(128)} %fb_ref.1) | copy-start | bytes 52
  13.8 0.7 %copy-start.13 = (f32[1,4]{1,0:T(1,128)S(1)}, f32[1,4]{1,0:T(1,128)}, u32[]{:S(2)}) copy-start(f32[1,4]{1,0:T(1,128)} %max_ref.1) | copy-start | bytes 52
  14.4 0.7 %copy-start.14 = (s32[1,2]{1,0:T(1,128)S(1)}, s32[1,2]{1,0:T(1,128)}, u32[]{:S(2)}) copy-start(s32[1,2]{1,0:T(1,128)} %member_ref.1) | copy-start | bytes 28
  15.1 0.7 %copy-start.15 = (f32[1,2]{1,0:T(1,128)S(1)}, f32[1,2]{1,0:T(1,128)}, u32[]{:S(2)}) copy-start(f32[1,2]{1,0:T(1,128)} %mw_ref.1) | copy-start | bytes 28

commit v2 on v1

--- a/solution.py
+++ b/solution.py
@@ -18,33 +18,41 @@
     n,
     cols,
     members,
-    tokens_ref,
-    gain_ref,
-    egain_ref,
+    tokens_hbm,
+    gain_hbm,
+    egain_hbm,
     q_hbm,
     k_hbm,
     v_hbm,
     o_hbm,
-    iw_ref,
-    fw_ref,
-    fb_ref,
+    iw_hbm,
+    fw_hbm,
+    fb_hbm,
     mem_hbm,
-    norm_ref,
-    max_ref,
+    norm_hbm,
+    max_hbm,
     mo_hbm,
     gate_hbm,
     up_hbm,
     down_hbm,
     group_ref,
-    member_ref,
+    member_hbm,
     gw_ref,
-    mw_ref,
+    mw_hbm,
     out_ref,
+    nmat_ref,
     nnorm_ref,
     nmax_ref,
-    key_ref,
-    av_ref,
-    keep_ref,
+    tokens_ref,
+    gain_ref,
+    egain_ref,
+    iw_ref,
+    fw_ref,
+    fb_ref,
+    norm_ref,
+    max_ref,
+    member_ref,
+    mw_ref,
     w_in,
     w_out,
     mem,
@@ -83,10 +91,20 @@
 
     loads = []
     for src, dst in (
+        (tokens_hbm, tokens_ref),
+        (gain_hbm, gain_ref),
+        (iw_hbm, iw_ref),
+        (fw_hbm, fw_ref),
+        (fb_hbm, fb_ref),
+        (max_hbm, max_ref),
         (q_hbm, w_in.at[pl.ds(0, cols)]),
         (k_hbm, w_in.at[pl.ds(cols, cols)]),
         (v_hbm, w_in.at[pl.ds(2 * cols, cols)]),
         (o_hbm, w_in.at[pl.ds(3 * cols, cols)]),
+        (norm_hbm, norm_ref),
+        (egain_hbm, egain_ref),
+        (member_hbm, member_ref),
+        (mw_hbm, mw_ref),
         (mem_hbm, mem),
         (mo_hbm, w_out),
         (gate_hbm, w_gate),
@@ -107,9 +125,11 @@
 
     lax.fori_loop(1, n, greet, 0)
 
+    half = me // (n // 2)
+
     def send_all(phase, source, target):
         def one(i, carry):
-            peer = lax.rem(me + i, n)
+            peer = lax.rem(me + half * i + (1 - half) * (n - i), n)
             pltpu.make_async_remote_copy(
                 src_ref=source(peer),
                 dst_ref=target.at[me],
@@ -133,6 +153,7 @@
             device_id_type=MESH,
         )
 
+    loads[0].wait()
     tok = tokens_ref[...].astype(f32)
     for s in range(blocks):
         row16[pl.ds(s, 1), :] = tok[:, s * LANES : (s + 1) * LANES]
@@ -142,6 +163,8 @@
     pl.semaphore_wait(barrier, n - 1)
     send_all(0, lambda peer: sb1, rb1)
 
+    for copy in loads[1:6]:
+        copy.wait()
     own = row16[...]
     scale = lax.rsqrt(
         jnp.sum(jnp.sum(own * own, axis=1, keepdims=True), axis=0, keepdims=True) / width + norm_eps
@@ -172,7 +195,6 @@
         jnp.int32, (heads, heads), 1
     )
     nmax_ref[...] = jnp.sum(jnp.where(diag, next_max, 0.0), axis=0, keepdims=True)
-    keep_ref[...] = jnp.broadcast_to(keep, (heads, LANES))
 
     r_index = lax.broadcasted_iota(jnp.int32, (pad4, head_dim), 0)
     j_index = lax.broadcasted_iota(jnp.int32, (pad4, head_dim), 1)
@@ -184,7 +206,7 @@
     if pad4 != 4 * cols:
         w_in[pl.ds(4 * cols, pad4 - 4 * cols), :] = jnp.zeros((pad4 - 4 * cols, width), bf16)
 
-    for copy in loads[:4]:
+    for copy in loads[6:10]:
         copy.wait()
     whole(0, rb1).wait_recv()
     rows = rb1[...].astype(f32)
@@ -200,13 +222,15 @@
     rb2[pl.ds(me, 1)] = sb2[pl.ds(me, 1)]
     send_all(1, lambda peer: sb2.at[peer], rb2)
 
-    loads[4].wait()
+    loads[14].wait()
     for h in range(heads):
         block = mem[h]
         high = block.astype(bf16)
         mem_hi[h] = high
         mem_lo[h] = (block - high.astype(f32)).astype(bf16)
 
+    for copy in loads[10:14]:
+        copy.wait()
     whole(1, rb2).wait_recv()
     for d in range(n):
         x2[pl.ds(d, 1), :] = rb2[d]
@@ -251,10 +275,15 @@
     rb3[pl.ds(me, 1)] = sb3[...][None]
     send_all(2, lambda peer: sb3, rb3)
     nnorm_ref[...] = keep * old_norm + admit * key
-    key_ref[...] = key
-    av_ref[...] = admit * value
-
-    loads[5].wait()
+    added = admit * value
+    for h in range(heads):
+        column = jnp.transpose(jnp.broadcast_to(added[h : h + 1, :], (LANES, head_dim)))
+        kept = jnp.broadcast_to(keep[h : h + 1, :], (head_dim, LANES))
+        for b in range(per):
+            span = slice(b * LANES, (b + 1) * LANES)
+            nmat_ref[h, :, span] = kept * mem[h, :, span] + column * key[h : h + 1, span]
+
+    loads[15].wait()
     whole(2, rb3).wait_recv()
     flat[...] = rb3[...].astype(f32).reshape(n * blocks, LANES)
     for s in range(blocks):
@@ -292,7 +321,7 @@
     for s in range(blocks):
         span = slice(s * LANES, (s + 1) * LANES)
         lhs[:, span] = (middle[:, span] * inverse * egain_ref[pl.ds(s, 1), :]).astype(bf16)
-    for copy in loads[6:]:
+    for copy in loads[16:]:
         copy.wait()
     gate_part = jnp.dot(lhs[...], w_gate[...], preferred_element_type=f32)
     up_part = jnp.dot(lhs[...], w_up[...], preferred_element_type=f32)
@@ -322,6 +351,22 @@
     whole(2, rb3).wait_send()
     whole(3, rb4).wait_send()
     whole(4, rb5).wait_send()
+
+
+def store(heads, row, mat, nrm, top, row_out, mat_out, nrm_out, top_out, sem):
+    pairs = [(mat.at[h], mat_out.at[h]) for h in range(heads)]
+    pairs += [(row, row_out), (nrm, nrm_out), (top, top_out)]
+    copies = [
+        pltpu.make_async_copy(src, dst, sem.at[i]) for i, (src, dst) in enumerate(pairs)
+    ]
+    for copy in copies:
+        copy.start()
+    for copy in copies:
+        copy.wait()
+
+
+def pin(x):
+    return pltpu.with_memory_space_constraint(x, pltpu.HBM)
 
 
 def local(
@@ -357,26 +402,31 @@
     members = n * expert_gate.shape[0] // GROUPS
     pad4 = -(-4 * cols // LANES) * LANES
     fold = LANES // cols
-    f32, bf16 = jnp.float32, jnp.bfloat16
+    f32, bf16, i32 = jnp.float32, jnp.bfloat16, jnp.int32
     vmem = pl.BlockSpec(memory_space=pltpu.VMEM)
     smem = pl.BlockSpec(memory_space=pltpu.SMEM)
-    anym = pl.BlockSpec(memory_space=pl.ANY)
+    hbm = pl.BlockSpec(memory_space=pltpu.HBM)
     outs = pl.pallas_call(
         functools.partial(kernel, n, cols, members),
         out_shape=(
             jax.ShapeDtypeStruct((1, width), bf16),
+            jax.ShapeDtypeStruct((heads, head_dim, head_dim), f32),
             jax.ShapeDtypeStruct((heads, head_dim), f32),
             jax.ShapeDtypeStruct((1, heads), f32),
-            jax.ShapeDtypeStruct((heads, head_dim), f32),
-            jax.ShapeDtypeStruct((heads, head_dim), f32),
-            jax.ShapeDtypeStruct((heads, LANES), f32),
         ),
-        in_specs=[vmem] * 3
-        + [anym] * 4
-        + [vmem, vmem, smem, anym, vmem, smem, anym, anym, anym, anym]
-        + [smem] * 4,
-        out_specs=(vmem,) * 6,
+        in_specs=[hbm] * 17 + [smem, hbm, smem, hbm],
+        out_specs=(vmem,) * 4,
         scratch_shapes=[
+            pltpu.VMEM((1, width), bf16),
+            pltpu.VMEM((blocks, LANES), f32),
+            pltpu.VMEM((blocks, LANES), f32),
+            pltpu.VMEM((heads, width), bf16),
+            pltpu.VMEM((heads, width), bf16),
+            pltpu.SMEM((heads,), f32),
+            pltpu.VMEM((heads, head_dim), f32),
+            pltpu.SMEM((1, heads), f32),
+            pltpu.SMEM((1, route_member.shape[1]), i32),
+            pltpu.SMEM((1, route_member.shape[1]), f32),
             pltpu.VMEM((pad4, width), bf16),
             pltpu.VMEM((cols, width), bf16),
             pltpu.VMEM((heads, head_dim, head_dim), f32),
@@ -401,7 +451,7 @@
             pltpu.VMEM((n * blocks, LANES), f32),
             pltpu.VMEM((n, width), bf16),
             pltpu.VMEM((n, width), f32),
-            pltpu.SemaphoreType.DMA((9,)),
+            pltpu.SemaphoreType.DMA((19,)),
             pltpu.SemaphoreType.DMA((5,)),
             pltpu.SemaphoreType.DMA((5,)),
         ],
@@ -409,34 +459,37 @@
             collective_id=0, has_side_effects=True, vmem_limit_bytes=48 * 1024 * 1024
         ),
     )(
-        tokens,
-        mixer_gain.reshape(blocks, LANES),
-        expert_gain.reshape(blocks, LANES),
-        query_weight.T,
-        key_weight.T,
-        value_weight.T,
-        outgate_weight.T,
-        input_weight.T,
-        forget_weight.T,
-        forget_bias,
-        memory_matrix[0],
-        memory_norm[0],
-        memory_max,
-        mixer_out.T,
-        expert_gate[0],
-        expert_up[0],
-        expert_down[0],
+        pin(tokens),
+        pin(mixer_gain.reshape(blocks, LANES)),
+        pin(expert_gain.reshape(blocks, LANES)),
+        pin(query_weight.T),
+        pin(key_weight.T),
+        pin(value_weight.T),
+        pin(outgate_weight.T),
+        pin(input_weight.T),
+        pin(forget_weight.T),
+        pin(forget_bias),
+        pin(memory_matrix[0]),
+        pin(memory_norm[0]),
+        pin(memory_max),
+        pin(mixer_out.T),
+        pin(expert_gate[0]),
+        pin(expert_up[0]),
+        pin(expert_down[0]),
         route_group,
-        route_member,
+        pin(route_member),
         group_weight,
-        member_weight,
-    )
-    layer_out, next_norm, next_max, key, value, keep = outs
-    next_matrix = (
-        keep[None, :, :1, None] * memory_matrix
-        + value[None, :, :, None] * key[None, :, None, :]
-    )
-    return (layer_out, next_matrix, next_norm[None], next_max)
+        pin(member_weight),
+    )
+    layer_out, next_matrix, next_norm, next_max = pl.pallas_call(
+        functools.partial(store, heads),
+        out_shape=tuple(jax.ShapeDtypeStruct(o.shape, o.dtype) for o in outs),
+        in_specs=[vmem] * 4,
+        out_specs=(hbm,) * 4,
+        scratch_shapes=[pltpu.SemaphoreType.DMA((heads + 3,))],
+        compiler_params=pltpu.CompilerParams(vmem_limit_bytes=1024 * 1024),
+    )(*outs)
+    return (layer_out, next_matrix[None], next_norm[None], next_max)
 
 
 def solution(mesh):

time: 59.2 us -> 41.3 us (0.70)
  local copies, waits for them, and re-layouts: 15.6 us -> 0 us
  other arithmetic: 2.57 us -> 0 us
  Pallas kernels: 38.4 us -> 39.1 us
    unnamed x35 -> x0, local copies, waits for them, and re-layouts: 15.5 us -> none
    add x1 -> x0, other arithmetic: 2.57 us -> none  [local(): keep[None, :, :1, None] * memory_matrix]
    pallas_call x0 -> x1, Pallas kernels: none -> 2.08 us  [local(): pl.pallas_call(functools.partial(store, heads), out_shape=tuple((jax.Shap...]
    pallas_call x1, Pallas kernels: 38.4 us -> 37 us  [local(): pl.pallas_call(functools.partial(kernel, n, cols, members), out_shape=(ja...]
where the time goes in v2:
time: 41.3 us; the launch traced here: 41 us
  Pallas kernels  39.1 us (95%)
  between operations  1.94 us (5%)
    pallas_call x1, Pallas kernels, local(): pl.pallas_call(functools.partial(kernel, n, cols, members), out_shape=(ja...  37 us
    pallas_call x1, Pallas kernels, local(): pl.pallas_call(functools.partial(store, heads), out_shape=tuple((jax.Shap...  2.08 us

profile of v2, /device:TPU:0, one launch (start us, length us, event | category | flops | bytes accessed | tf_op | source)
XLA Modules:
  0.0 41.0 jit_solution(4190971485921048559)
XLA Ops:
  1.9 37.0 %shard_map.228 = (bf16[1,2048]{1,0:T(2,128)(2,1)S(1)}, f32[4,512,512]{2,1,0:T(8,128)S(1)}, f32[4,512]{1,0:T(4,128)S(1)}, f32[1,4]{1,0:T(1,128)S(1)}) custom-call(bf16[1,2048]{1,0:T(2,128)(2,1)} %tokens_hbm.1, f32[16,128]{1,0:T(8,128)} %bitcast.27, f32[16,128]{1,0:T(8,128)} %bitcast.28, bf16[64,2048]{1,0:T(8,128)(2,1)} %bitcast.20, ...), custom_call_target="tpu_custom_call" | custom-call | tf_op jit(solution)/shard_map/pallas_call | solution.py:409
  38.9 2.1 %shard_map.229 = (bf16[1,2048]{1,0:T(2,128)(2,1)}, f32[4,512,512]{2,1,0:T(8,128)}, f32[4,512]{1,0:T(4,128)}, f32[1,4]{1,0:T(1,128)}) custom-call(bf16[1,2048]{1,0:T(2,128)(2,1)S(1)} %get-tuple-element.12.row, f32[4,512,512]{2,1,0:T(8,128)S(1)} %get-tuple-element.13.mat, f32[4,512]{1,0:T(4,128)S(1)} %get-tuple-element.14.nrm, f32[1,4]{1,0:T(1,128)S(1)} %get-tuple-element.15.top), custom_call_target="tpu_custom_call" | custom-call | tf_op jit(solution)/shard_map/pallas_call | solution.py:484

commit v3 on v2

--- a/solution.py
+++ b/solution.py
@@ -89,6 +89,30 @@
     f32 = jnp.float32
     bf16 = jnp.bfloat16
 
+    half = me // (n // 2)
+    first = me + (1 - half) * n
+    turn = 2 * half - 1
+
+    def each_peer(body):
+        chunk = 8
+        full = (n - 1) // chunk
+
+        def several(k, carry):
+            for u in range(chunk):
+                body(lax.rem(first + turn * (k * chunk + u + 1), n))
+            return carry
+
+        lax.fori_loop(0, full, several, 0)
+        for u in range(full * chunk + 1, n):
+            body(lax.rem(first + turn * u, n))
+
+    barrier = pltpu.get_barrier_semaphore()
+
+    def greet(peer):
+        pl.semaphore_signal(barrier, inc=1, device_id=(peer,), device_id_type=MESH)
+
+    each_peer(greet)
+
     loads = []
     for src, dst in (
         (tokens_hbm, tokens_ref),
@@ -115,21 +139,8 @@
         copy.start()
         loads.append(copy)
 
-    barrier = pltpu.get_barrier_semaphore()
-
-    def greet(i, carry):
-        pl.semaphore_signal(
-            barrier, inc=1, device_id=(lax.rem(me + i, n),), device_id_type=MESH
-        )
-        return carry
-
-    lax.fori_loop(1, n, greet, 0)
-
-    half = me // (n // 2)
-
     def send_all(phase, source, target):
-        def one(i, carry):
-            peer = lax.rem(me + half * i + (1 - half) * (n - i), n)
+        def one(peer):
             pltpu.make_async_remote_copy(
                 src_ref=source(peer),
                 dst_ref=target.at[me],
@@ -138,9 +149,8 @@
                 device_id=(peer,),
                 device_id_type=MESH,
             ).start()
-            return carry
-
-        lax.fori_loop(1, n, one, 0)
+
+        each_peer(one)
 
     def whole(phase, target):
         view = target.at[pl.ds(0, n - 1)]
@@ -219,8 +229,8 @@
     result = result.astype(bf16).astype(f32)
     for t in range(n):
         sb2[t] = result[t : t + 1, :]
+    send_all(1, lambda peer: sb2.at[peer], rb2)
     rb2[pl.ds(me, 1)] = sb2[pl.ds(me, 1)]
-    send_all(1, lambda peer: sb2.at[peer], rb2)
 
     loads[14].wait()
     for h in range(heads):
@@ -272,8 +282,8 @@
     for b in range(per):
         row16[pl.ds(b, heads, stride=per), :] = gated[:, b * LANES : (b + 1) * LANES]
     sb3[...] = row16[...].astype(bf16)
+    send_all(2, lambda peer: sb3, rb3)
     rb3[pl.ds(me, 1)] = sb3[...][None]
-    send_all(2, lambda peer: sb3, rb3)
     nnorm_ref[...] = keep * old_norm + admit * key
     added = admit * value
     for h in range(heads):
@@ -295,8 +305,8 @@
     sb4[...] = jnp.concatenate(
         [proj[f * piece : (f + 1) * piece, :] for f in range(fold)], axis=1
     ).astype(bf16)
+    send_all(3, lambda peer: sb4, rb4)
     rb4[pl.ds(me, 1)] = sb4[...][None]
-    send_all(3, lambda peer: sb4, rb4)
     flat[...] = rb1[...].astype(f32).reshape(n * blocks, LANES)
 
     whole(3, rb4).wait_recv()
@@ -330,8 +340,8 @@
     for s in range(blocks):
         flat[pl.ds(s, n, stride=blocks), :] = finished[:, s * LANES : (s + 1) * LANES]
     sb5[...] = flat[...].astype(bf16).reshape(n, blocks, LANES)
+    send_all(4, lambda peer: sb5.at[peer], rb5)
     rb5[pl.ds(me, 1)] = sb5[pl.ds(me, 1)]
-    send_all(4, lambda peer: sb5.at[peer], rb5)
 
     own_middle = middle[pl.ds(me, 1), :]
     for s in range(blocks):

time: 41.3 us -> 40.9 us (level)
  no operation moved by 1% of the time
where the time goes in v3:
time: 40.9 us; the launch traced here: 40.6 us
  Pallas kernels  38.7 us (95%)
  between operations  1.94 us (5%)
    pallas_call x1, Pallas kernels, local(): pl.pallas_call(functools.partial(kernel, n, cols, members), out_shape=(ja...  36.6 us
    pallas_call x1, Pallas kernels, local(): pl.pallas_call(functools.partial(store, heads), out_shape=tuple((jax.Shap...  2.08 us

profile of v3, /device:TPU:0, one launch (start us, length us, event | category | flops | bytes accessed | tf_op | source)
XLA Modules:
  0.0 40.6 jit_solution(10697473771876910151)
XLA Ops:
  1.9 36.6 %shard_map.228 = (bf16[1,2048]{1,0:T(2,128)(2,1)S(1)}, f32[4,512,512]{2,1,0:T(8,128)S(1)}, f32[4,512]{1,0:T(4,128)S(1)}, f32[1,4]{1,0:T(1,128)S(1)}) custom-call(bf16[1,2048]{1,0:T(2,128)(2,1)} %tokens_hbm.1, f32[16,128]{1,0:T(8,128)} %bitcast.27, f32[16,128]{1,0:T(8,128)} %bitcast.28, bf16[64,2048]{1,0:T(8,128)(2,1)} %bitcast.20, ...), custom_call_target="tpu_custom_call" | custom-call | tf_op jit(solution)/shard_map/pallas_call | solution.py:419
  38.6 2.1 %shard_map.229 = (bf16[1,2048]{1,0:T(2,128)(2,1)}, f32[4,512,512]{2,1,0:T(8,128)}, f32[4,512]{1,0:T(4,128)}, f32[1,4]{1,0:T(1,128)}) custom-call(bf16[1,2048]{1,0:T(2,128)(2,1)S(1)} %get-tuple-element.12.row, f32[4,512,512]{2,1,0:T(8,128)S(1)} %get-tuple-element.13.mat, f32[4,512]{1,0:T(4,128)S(1)} %get-tuple-element.14.nrm, f32[1,4]{1,0:T(1,128)S(1)} %get-tuple-element.15.top), custom_call_target="tpu_custom_call" | custom-call | tf_op jit(solution)/shard_map/pallas_call | solution.py:494
